TPU v7x, 256 devices: a whole 4x4x8 slice. The times are simulated.
256 devices in a mesh: fs: 32 (over z, y), tp: 8 (over x, core).
Axes of the slice: x: 4, y: 4, z: 8, core: 2. Of those that a mesh axis runs over, the one named last changes fastest.
Arguments:
- tokens: bfloat16 [12288, 2048], P(('fs', 'tp')), may hold values from -6 to 6
- ffn1_gain: float32 [2048], replicated, may hold values from 0.1 to 1.9
- ffn1_gate: bfloat16 [2048, 5632], P('fs', 'tp'), may hold values from -0.125 to 0.125
- ffn1_up: bfloat16 [2048, 5632], P('fs', 'tp'), may hold values from -0.125 to 0.125
- ffn1_down: bfloat16 [5632, 2048], P('tp', 'fs'), may hold values from -0.078125 to 0.078125
- mix_gain: float32 [2048], replicated, may hold values from 0.1 to 1.9
- lru_in_weight: bfloat16 [2048, 1536], P('fs', 'tp'), may hold values from -0.125 to 0.125
- lru_gate_weight: bfloat16 [2048, 1536], P('fs', 'tp'), may hold values from -0.125 to 0.125
- conv_weight: bfloat16 [4, 1536], P(None, 'tp'), may hold values from -3 to 3
- gate_a_weight: bfloat16 [24, 64, 64], P('tp'), may hold values from -0.75 to 0.75
- gate_x_weight: bfloat16 [24, 64, 64], P('tp'), may hold values from -0.75 to 0.75
- decay_param: float32 [1536], P('tp'), may hold values from 3.7 to 9
- mix_out_weight: bfloat16 [1536, 2048], P('tp', 'fs'), may hold values from -0.15625 to 0.15625
- ffn2_gain: float32 [2048], replicated, may hold values from 0.1 to 1.9
- ffn2_gate: bfloat16 [2048, 5632], P('fs', 'tp'), may hold values from -0.125 to 0.125
- ffn2_up: bfloat16 [2048, 5632], P('fs', 'tp'), may hold values from -0.125 to 0.125
- ffn2_down: bfloat16 [5632, 2048], P('tp', 'fs'), may hold values from -0.078125 to 0.078125
Outputs:
- layer_out: bfloat16 [12288, 2048], P(('fs', 'tp'))
All inputs are finite; a program needn't handle non-finite values.
Results may differ from a plain program's by a relative error of at most 0.017.
Values may be sent and summed in bfloat16 or wider, within the bound.
No kernel may reach another device: no remote copies, remote signals or barrier semaphores. Data moves between devices by JAX's collectives and lax.ppermute only.
A program may use at most 64 MiB of HBM per device.

v0:
```python
import jax
import jax.numpy as jnp
from jax import lax
from jax.sharding import Mesh
from jax.sharding import PartitionSpec as P

FS = ("fs_0", "fs_1")
FS_TP = ("fs_0", "fs_1", "tp")


EPS = 1e-06


def joined_along(blocks, dim):
    dims = list(blocks.shape[1:])
    dims[dim] *= blocks.shape[0]
    return jnp.moveaxis(blocks, 0, dim).reshape(dims)


def sent_to_all(value, axis):
    copies = jnp.broadcast_to(value, (lax.axis_size(axis), *value.shape))
    return lax.all_to_all(copies, axis, split_axis=0, concat_axis=0, tiled=True)


def gathered_copies(value, axis, dim):
    return joined_along(sent_to_all(value, axis), dim)


def sent_together(arrays, axis, dim, along):
    ends, at = ([], 0)
    for a in arrays[:-1]:
        at += a.shape[along]
        ends.append(at)
    both = jnp.concatenate(arrays, axis=along)
    return tuple(jnp.split(lax.all_gather(both, axis, axis=dim, tiled=True), ends, axis=along))


def gathered_by_axis(value, axes, dim):
    for axis in reversed(axes):
        value = lax.all_gather(value, axis, axis=dim, tiled=True)
    return value


def in_blocks(value, dim, length):
    before, after = (value.shape[:dim], value.shape[dim + 1 :])
    return jnp.moveaxis(value.reshape(*before, length, -1, *after), dim, 0)


def sent_and_summed(value, axis, dim):
    blocks = in_blocks(value, dim, lax.axis_size(axis))
    arrived = lax.all_to_all(blocks, axis, split_axis=0, concat_axis=0, tiled=True)
    return arrived.astype(jnp.float32).sum(axis=0)


def rms_rows(values, gain):
    wide = values.astype(jnp.float32)
    scale = lax.rsqrt(jnp.mean(wide * wide, axis=-1, keepdims=True) + EPS)
    return (wide * scale * gain).astype(jnp.bfloat16)


def gather_rows(values):
    return gathered_copies(values, "tp", 0)


def pair_step(rows, pieces):
    return (
        jnp.dot(rows, pieces[0], preferred_element_type=jnp.float32),
        jnp.dot(rows, pieces[1], preferred_element_type=jnp.float32),
    )


def block_hidden(rows, gate_weight, up_weight):
    gate, upper = pair_step(rows, sent_together((gate_weight, up_weight), FS, 0, 1))
    return (jax.nn.silu(gate) * upper).astype(jnp.bfloat16)


def block_terms(hidden, down_weight):
    return jnp.dot(hidden, gathered_by_axis(down_weight, FS, 1), preferred_element_type=jnp.float32)


def reduce_rows(terms):
    return sent_and_summed(terms.astype(jnp.bfloat16), "tp", 0)


def combine(earlier, later):
    return (earlier[0] * later[0], later[0] * earlier[1] + later[1])


def mixer_terms(
    rows,
    lru_in_weight,
    lru_gate_weight,
    conv_weight,
    gate_a_weight,
    gate_x_weight,
    decay_param,
    mix_out_weight,
):
    lru_x, lru_gate = pair_step(rows, sent_together((lru_in_weight, lru_gate_weight), FS, 0, 1))
    lru_low = lru_x.astype(jnp.bfloat16).astype(jnp.float32)
    gate_low = lru_gate.astype(jnp.bfloat16).astype(jnp.float32)
    length = rows.shape[0]
    taps_count = conv_weight.shape[0]
    padded = jnp.pad(lru_low, ((taps_count - 1, 0), (0, 0)))
    taps = conv_weight.astype(jnp.float32)
    conv = jnp.zeros_like(lru_low)
    for offset in range(taps_count):
        conv = (
            conv + taps[offset] * padded[taps_count - 1 - offset : taps_count - 1 - offset + length]
        )
    conv_low = conv.astype(jnp.bfloat16)
    blocks = conv_low.reshape(length, gate_a_weight.shape[0], gate_a_weight.shape[1])
    recall = jax.nn.sigmoid(
        jnp.einsum(
            "sbi,bij->sbj", blocks, gate_a_weight, preferred_element_type=jnp.float32
        ).reshape(length, -1)
    )
    admit = jax.nn.sigmoid(
        jnp.einsum(
            "sbi,bij->sbj", blocks, gate_x_weight, preferred_element_type=jnp.float32
        ).reshape(length, -1)
    )
    log_keep = -8.0 * recall * jax.nn.softplus(-decay_param)
    drive = jnp.sqrt(-jnp.expm1(2.0 * log_keep)) * admit * conv_low.astype(jnp.float32)
    _, state = lax.associative_scan(combine, (jnp.exp(log_keep), drive), axis=0)
    mixed = (state * jax.nn.gelu(gate_low)).astype(jnp.bfloat16)
    return jnp.dot(
        mixed, gathered_copies(mix_out_weight, FS, 1), preferred_element_type=jnp.float32
    )


def body(
    tokens,
    ffn1_gain,
    ffn1_gate,
    ffn1_up,
    ffn1_down,
    mix_gain,
    lru_in_weight,
    lru_gate_weight,
    conv_weight,
    gate_a_weight,
    gate_x_weight,
    decay_param,
    mix_out_weight,
    ffn2_gain,
    ffn2_gate,
    ffn2_up,
    ffn2_down,
):
    rows = gather_rows(rms_rows(tokens, ffn1_gain))
    terms = block_terms(block_hidden(rows, ffn1_gate, ffn1_up), ffn1_down)
    first = (tokens.astype(jnp.float32) + 0.5 * reduce_rows(terms)).astype(jnp.bfloat16)
    rows = gather_rows(rms_rows(first, mix_gain))
    terms = mixer_terms(
        rows,
        lru_in_weight,
        lru_gate_weight,
        conv_weight,
        gate_a_weight,
        gate_x_weight,
        decay_param,
        mix_out_weight,
    )
    second = (first.astype(jnp.float32) + reduce_rows(terms)).astype(jnp.bfloat16)
    rows = gather_rows(rms_rows(second, ffn2_gain))
    terms = block_terms(block_hidden(rows, ffn2_gate, ffn2_up), ffn2_down)
    return (second.astype(jnp.float32) + 0.5 * reduce_rows(terms)).astype(jnp.bfloat16)


def solution(mesh):
    split = Mesh(mesh.devices.reshape(8, 4, mesh.shape["tp"]), ("fs_0", "fs_1", "tp"))
    placed = (
        P(FS_TP, None),
        P(),
        P(FS, "tp"),
        P(FS, "tp"),
        P("tp", FS),
        P(),
        P(FS, "tp"),
        P(FS, "tp"),
        P(None, "tp"),
        P("tp", None, None),
        P("tp", None, None),
        P("tp"),
        P("tp", FS),
        P(),
        P(FS, "tp"),
        P(FS, "tp"),
        P("tp", FS),
    )
    return jax.shard_map(
        body, mesh=split, in_specs=placed, out_specs=P(FS_TP, None), check_vma=False
    )
```

profile of v0, /device:TPU:1, one launch (start us, length us, event | category | flops | bytes accessed | tf_op | source)
XLA Modules:
  0.0 395.7 jit_solution(10681812931382943686)
XLA Ops:
  6.6 1.8 pad_maximum_fusion.1
  8.5 13.0 %all_gather.22 = bf16[704,256]{0,1:T(8,128)(2,1)} all-gather(bf16[704,64]{0,1:T(8,128)(2,1)} %param.21), channel_id=1, replica_groups=mesh['fs_0'=8,'fs_1'=4,'tp'=8] {'fs_1'}, dimensions={1}, use_global_device_ids=true | all-gather | bytes 450560 | tf_op jit(solution)/shard_map/all_gather | solution.py:40
  24.4 27.9 %all_to_all.35 = bf16[8,48,2048]{2,1,0:T(8,128)(2,1)S(1)} all-to-all(bf16[8,48,2048]{2,1,0:T(8,128)(2,1)S(1)} %broadcast_in_dim.8), channel_id=1, replica_groups=mesh['fs_0'=8,'fs_1'=4,'tp'=8] {'tp'}, dimensions={0} | all-to-all | bytes 3145728 | tf_op jit(solution)/shard_map/all_to_all | solution.py:22
  52.3 46.3 %all-gather.6.cloned.1.call-done = bf16[2048,1408]{1,0:T(8,128)(2,1)} async-done(((bf16[64,1408]{1,0:T(8,128)(2,1)}), bf16[2048,1408]{1,0:T(8,128)(2,1)}) %all-gather.6.cloned.1.call-update) | async-done | bytes 5767184 | tf_op jit(solution)/shard_map/all_gather | solution.py:35
  98.6 3.6 fusion.6
  102.1 41.2 %all-gather.8.cloned.1.call-done = bf16[704,2048]{0,1:T(8,128)(2,1)} async-done(((bf16[704,256]{0,1:T(8,128)(2,1)}), bf16[704,2048]{0,1:T(8,128)(2,1)}) %all-gather.8.cloned.1.call-update) | async-done | bytes 2883600 | tf_op jit(solution)/shard_map/all_gather | solution.py:40
  143.3 8.3 %convolution_convert_fusion.1 = bf16[384,2048]{1,0:T(8,128)(2,1)} fusion(bf16[704,2048]{0,1:T(8,128)(2,1)} %all-gather.8.cloned.1.call-done, bf16[384,2048]{1,0:T(8,128)(2,1)S(1)} %bitcast.38, bf16[2048,1408]{1,0:T(8,128)(2,1)} %all-gather.6.cloned.1.call-done, f32[384,704]{0,1:T(8,128)S(1)} %fusion.6), kind=kOutput, calls=%fused_computation.12 | convolution fusion | flops 2217000960 | bytes 10518528 | tf_op jit(solution)/shard_map/dot_general | solution.py:78
  151.6 26.0 %all_to_all.36 = bf16[8,48,2048]{2,1,0:T(8,128)(2,1)S(1)} all-to-all(bf16[8,48,2048]{2,1,0:T(8,128)(2,1)} %bitcast.40), channel_id=1, replica_groups=mesh['fs_0'=8,'fs_1'=4,'tp'=8] {'tp'}, dimensions={0} | all-to-all | bytes 3145728 | tf_op jit(solution)/shard_map/all_to_all | solution.py:51
  179.8 4.7 %all-to-all-start.2 = ((bf16[8,48,2048]{2,1,0:T(8,128)(2,1)}), bf16[8,48,2048]{2,1,0:T(8,128)(2,1)S(1)}, u32[]{:S(2)}, u32[]{:S(2)}) async-start(bf16[8,48,2048]{2,1,0:T(8,128)(2,1)} %broadcast_in_dim.9), calls=%async_computation.2 | async-start | bytes 3145728 | tf_op jit(solution)/shard_map/all_to_all | solution.py:22
  184.5 11.3 %all_gather.26 = bf16[704,256]{0,1:T(8,128)(2,1)} all-gather(bf16[704,64]{0,1:T(8,128)(2,1)S(1)} %copy-done.4), channel_id=1, replica_groups=mesh['fs_0'=8,'fs_1'=4,'tp'=8] {'fs_1'}, dimensions={1}, use_global_device_ids=true | all-gather | bytes 450560 | tf_op jit(solution)/shard_map/all_gather | solution.py:40
  195.8 9.3 %all-to-all-done.2 = bf16[8,48,2048]{2,1,0:T(8,128)(2,1)S(1)} async-done(((bf16[8,48,2048]{2,1,0:T(8,128)(2,1)}), bf16[8,48,2048]{2,1,0:T(8,128)(2,1)S(1)}, u32[]{:S(2)}, u32[]{:S(2)}) %all-to-all-start.2) | async-done | bytes 1572896 | tf_op jit(solution)/shard_map/all_to_all | solution.py:22
  206.2 7.2 %all-to-all-start.3 = ((bf16[32,192,64]{1,2,0:T(8,128)(2,1)}), bf16[32,192,64]{1,2,0:T(8,128)(2,1)}, u32[]{:S(2)}, u32[]{:S(2)}) async-start(bf16[32,192,64]{1,2,0:T(8,128)(2,1)} %broadcast_in_dim.10), calls=%async_computation.3 | async-start | bytes 2097152 | tf_op jit(solution)/shard_map/all_to_all | solution.py:22
  213.4 4.2 %all-gather.10.cloned.1.call-done = bf16[2048,384]{1,0:T(8,128)(2,1)} async-done(((bf16[64,384]{1,0:T(8,128)(2,1)}), bf16[2048,384]{1,0:T(8,128)(2,1)}) %all-gather.10.cloned.1.call-update) | async-done | bytes 1572880 | tf_op jit(solution)/shard_map/all_gather | solution.py:35
  217.6 1.8 fusion.21
  231.4 1.6 pad.68
  233.0 6.8 %all-to-all-done.3 = bf16[32,192,64]{1,2,0:T(8,128)(2,1)} async-done(((bf16[32,192,64]{1,2,0:T(8,128)(2,1)}), bf16[32,192,64]{1,2,0:T(8,128)(2,1)}, u32[]{:S(2)}, u32[]{:S(2)}) %all-to-all-start.3) | async-done | bytes 786464 | tf_op jit(solution)/shard_map/all_to_all | solution.py:22
  239.8 3.7 convolution_convert_fusion.2
  243.5 25.9 %all_to_all.37 = bf16[8,48,2048]{2,1,0:T(8,128)(2,1)S(1)} all-to-all(bf16[8,48,2048]{2,1,0:T(8,128)(2,1)S(1)} %bitcast.39), channel_id=1, replica_groups=mesh['fs_0'=8,'fs_1'=4,'tp'=8] {'tp'}, dimensions={0} | all-to-all | bytes 3145728 | tf_op jit(solution)/shard_map/all_to_all | solution.py:51
  271.6 4.5 %all-to-all-start.5 = ((bf16[8,48,2048]{2,1,0:T(8,128)(2,1)}), bf16[8,48,2048]{2,1,0:T(8,128)(2,1)S(1)}, u32[]{:S(2)}, u32[]{:S(2)}) async-start(bf16[8,48,2048]{2,1,0:T(8,128)(2,1)} %broadcast_in_dim.22), calls=%async_computation.5 | async-start | bytes 3145728 | tf_op jit(solution)/shard_map/all_to_all | solution.py:22
  276.1 33.2 %all-gather.12.cloned.1.call-done = bf16[2048,1408]{1,0:T(8,128)(2,1)} async-done(((bf16[64,1408]{1,0:T(8,128)(2,1)}), bf16[2048,1408]{1,0:T(8,128)(2,1)}) %all-gather.12.cloned.1.call-update) | async-done | bytes 5767184 | tf_op jit(solution)/shard_map/all_gather | solution.py:35
  309.3 3.6 fusion.2
  312.9 41.0 %all-gather.14.cloned.1.call-done = bf16[704,2048]{0,1:T(8,128)(2,1)} async-done(((bf16[704,256]{0,1:T(8,128)(2,1)}), bf16[704,2048]{0,1:T(8,128)(2,1)}) %all-gather.14.cloned.1.call-update) | async-done | bytes 2883600 | tf_op jit(solution)/shard_map/all_gather | solution.py:40
  353.9 8.2 %convolution_convert_fusion = bf16[384,2048]{1,0:T(8,128)(2,1)} fusion(bf16[704,2048]{0,1:T(8,128)(2,1)} %all-gather.14.cloned.1.call-done, bf16[384,2048]{1,0:T(8,128)(2,1)S(1)} %bitcast.36, bf16[2048,1408]{1,0:T(8,128)(2,1)} %all-gather.12.cloned.1.call-done, f32[384,704]{0,1:T(8,128)S(1)} %fusion.2), kind=kOutput, calls=%fused_computation.11 | convolution fusion | flops 2217000960 | bytes 10518528 | tf_op jit(solution)/shard_map/dot_general | solution.py:78
  362.1 26.0 %all_to_all.38 = bf16[8,48,2048]{2,1,0:T(8,128)(2,1)S(1)} all-to-all(bf16[8,48,2048]{2,1,0:T(8,128)(2,1)} %bitcast.41), channel_id=1, replica_groups=mesh['fs_0'=8,'fs_1'=4,'tp'=8] {'tp'}, dimensions={0} | all-to-all | bytes 3145728 | tf_op jit(solution)/shard_map/all_to_all | solution.py:51
  (156 shorter events, 20.9 us)
Async XLA Ops:
  6.5 213.2 %copy-start = (bf16[3,64,64]{2,1,0:T(8,128)(2,1)S(1)}, bf16[3,64,64]{2,1,0:T(8,128)(2,1)}, u32[]{:S(2)}) copy-start(bf16[3,64,64]{2,1,0:T(8,128)(2,1)} %param.26) | copy-start | bytes 73732
  6.5 16.5 %copy-start.3 = (bf16[64,704]{1,0:T(8,128)(2,1)S(1)}, bf16[64,704]{1,0:T(8,128)(2,1)}, u32[]{:S(2)}) copy-start(bf16[64,704]{1,0:T(8,128)(2,1)} %param.31) | copy-start | bytes 270340
  6.5 16.5 %copy-start.2 = (bf16[64,704]{1,0:T(8,128)(2,1)S(1)}, bf16[64,704]{1,0:T(8,128)(2,1)}, u32[]{:S(2)}) copy-start(bf16[64,704]{1,0:T(8,128)(2,1)} %param.32) | copy-start | bytes 270340
  6.5 17.3 %copy-start.1 = (bf16[48,2048]{1,0:T(8,128)(2,1)S(1)}, bf16[48,2048]{1,0:T(8,128)(2,1)}, u32[]{:S(2)}) copy-start(bf16[48,2048]{1,0:T(8,128)(2,1)} %param.17) | copy-start | bytes 589828
  6.5 17.5 %copy-start.6 = (f32[2048]{0:T(1024)S(1)}, f32[2048]{0:T(1024)}, u32[]{:S(2)}) copy-start(f32[2048]{0:T(1024)} %param.18) | copy-start | bytes 24580
  6.5 92.0 %all-gather.6.cloned.1.call-start = ((), (), s32[]{:S(2)}) async-start(), calls=%async_computation.7 | async-start | bytes 5947392 | tf_op jit(solution)/shard_map/all_gather | solution.py:35
  8.4 134.9 %all-gather.8.cloned.1.call-start = ((), (), s32[]{:S(2)}) async-start(), calls=%async_computation.8 | async-start | bytes 3538944 | tf_op jit(solution)/shard_map/all_gather | solution.py:40
  21.5 196.1 %all-gather.10.cloned.1.call-start = ((), (), s32[]{:S(2)}) async-start(), calls=%async_computation.9 | async-start | bytes 1622016 | tf_op jit(solution)/shard_map/all_gather | solution.py:35
  23.0 286.3 %all-gather.12.cloned.1.call-start = ((), (), s32[]{:S(2)}) async-start(), calls=%async_computation.10 | async-start | bytes 5947392 | tf_op jit(solution)/shard_map/all_gather | solution.py:35
  177.6 0.7 copy-start.7
  179.8 4.7 %copy-start.4 = (bf16[704,64]{0,1:T(8,128)(2,1)S(1)}, bf16[704,64]{0,1:T(8,128)(2,1)}, u32[]{:S(2)}) copy-start(bf16[704,64]{0,1:T(8,128)(2,1)} %param.33) | copy-start | bytes 270340
  179.8 16.0 %copy-start.10 = (f32[192]{0:T(256)S(1)}, f32[192]{0:T(256)}, u32[]{:S(2)}) copy-start(f32[192]{0:T(256)} %param.28) | copy-start | bytes 2308
  179.8 16.0 %copy-start.9 = (bf16[4,192]{1,0:T(4,128)(2,1)S(1)}, bf16[4,192]{1,0:T(4,128)(2,1)}, u32[]{:S(2)}) copy-start(bf16[4,192]{1,0:T(4,128)(2,1)} %param.25) | copy-start | bytes 4612
  179.8 25.3 %copy-start.5 = (bf16[192,64]{0,1:T(8,128)(2,1)S(1)}, bf16[192,64]{0,1:T(8,128)(2,1)}, u32[]{:S(2)}) copy-start(bf16[192,64]{0,1:T(8,128)(2,1)} %param.29) | copy-start | bytes 73732
  179.8 25.3 %all-to-all-start.2 = ((bf16[8,48,2048]{2,1,0:T(8,128)(2,1)}), bf16[8,48,2048]{2,1,0:T(8,128)(2,1)S(1)}, u32[]{:S(2)}, u32[]{:S(2)}) async-start(bf16[8,48,2048]{2,1,0:T(8,128)(2,1)} %broadcast_in_dim.9), calls=%async_computation.2 | async-start | bytes 3145728 | tf_op jit(solution)/shard_map/all_to_all | solution.py:22
  184.5 169.4 %all-gather.14.cloned.1.call-start = ((), (), s32[]{:S(2)}) async-start(), calls=%async_computation.11 | async-start | bytes 3538944 | tf_op jit(solution)/shard_map/all_gather | solution.py:40
  206.2 33.6 %all-to-all-start.3 = ((bf16[32,192,64]{1,2,0:T(8,128)(2,1)}), bf16[32,192,64]{1,2,0:T(8,128)(2,1)}, u32[]{:S(2)}, u32[]{:S(2)}) async-start(bf16[32,192,64]{1,2,0:T(8,128)(2,1)} %broadcast_in_dim.10), calls=%async_computation.3 | async-start | bytes 2097152 | tf_op jit(solution)/shard_map/all_to_all | solution.py:22
  219.4 0.8 copy-start.11
  269.4 0.7 copy-start.8
  271.6 37.7 %all-to-all-start.5 = ((bf16[8,48,2048]{2,1,0:T(8,128)(2,1)}), bf16[8,48,2048]{2,1,0:T(8,128)(2,1)S(1)}, u32[]{:S(2)}, u32[]{:S(2)}) async-start(bf16[8,48,2048]{2,1,0:T(8,128)(2,1)} %broadcast_in_dim.22), calls=%async_computation.5 | async-start | bytes 3145728 | tf_op jit(solution)/shard_map/all_to_all | solution.py:22
Sparse Core Ops, SparseCore 0:
  9.9 88.5 all-gather.5
  100.3 42.9 all-gather.7
  145.9 71.6 all-gather.9
  220.0 89.2 all-gather.11
  310.9 42.9 all-gather.13
where the time goes:
time: 397 us; the launch traced here: 396 us
  waiting for transfers between devices  182 us (46%)
  blocking collectives  130 us (33%)
  matrix products  29.7 us (7%)
  starting transfers between devices  16.6 us (4%)
  between operations  13.8 us (3%)
  local copies, waits for them, and re-layouts  13.1 us (3%)
  other arithmetic  10.3 us (3%)
    all_gather x3, waiting for transfers between devices, sent_together(): lax.all_gather(both, axis, axis=dim, tiled=True)  83.6 us
    all_gather x2, waiting for transfers between devices, gathered_by_axis(): value = lax.all_gather(value, axis, axis=dim, tiled=True)  82.2 us
    all_to_all x3, blocking collectives, sent_and_summed(): lax.all_to_all(blocks, axis, split_axis=0, concat_axis=0, tiled=True)  78 us
    all_to_all x1, blocking collectives, sent_to_all(): return lax.all_to_all(copies, axis, split_axis=0, concat_axis=0, tiled=True)  27.9 us
    all_gather x2, blocking collectives, gathered_by_axis(): value = lax.all_gather(value, axis, axis=dim, tiled=True)  24.3 us
    dot_general x2, matrix products, block_terms(): jnp.dot(hidden, gathered_by_axis(down_weight, FS, 1), preferred_element_t...  16.5 us
    all_to_all x3, starting transfers between devices, sent_to_all(): return lax.all_to_all(copies, axis, split_axis=0, concat_axis=0, tiled=True)  16.4 us
    all_to_all x3, waiting for transfers between devices, sent_to_all(): return lax.all_to_all(copies, axis, split_axis=0, concat_axis=0, tiled=True)  16.1 us
  transfers between devices with their start and end apart: 8, of which 7 were waited for; matrix products, arithmetic and copies ran while one was open for 10% of the time, Pallas kernels for 0%

commit v1 on v0

v1 whole, which is shorter than its diff:
```python
import jax
import jax.numpy as jnp
from jax import lax
from jax.experimental import pallas as pl
from jax.experimental.pallas import tpu as pltpu
from jax.sharding import Mesh
from jax.sharding import PartitionSpec as P

FS = ("fs_0", "fs_1")
FS_TP = ("fs_0", "fs_1", "tp")

EPS = 1e-06
LANES = 128
SHARD = 64
HALF = 64


def rms_rows(values, gain):
    wide = values.astype(jnp.float32)
    scale = lax.rsqrt(jnp.mean(wide * wide, axis=-1, keepdims=True) + EPS)
    return (wide * scale * gain).astype(jnp.bfloat16)


def gather_rows(values):
    copies = jnp.broadcast_to(values, (lax.axis_size("tp"), *values.shape))
    arrived = lax.all_to_all(copies, "tp", split_axis=0, concat_axis=0, tiled=True)
    return arrived.reshape(-1, values.shape[-1])


def reduce_rows(terms):
    blocks = terms.reshape(lax.axis_size("tp"), -1, terms.shape[-1])
    arrived = lax.all_to_all(blocks, "tp", split_axis=0, concat_axis=0, tiled=True)
    return arrived.astype(jnp.float32).sum(axis=0)


def tiles_of(weight):
    return [weight[:, k : k + LANES] for k in range(0, weight.shape[1], LANES)]


def paired_tiles(first, second):
    whole = first.shape[1] // LANES * LANES
    ends = jnp.concatenate([first[:, whole:], second[:, whole:]], axis=1)
    return tiles_of(first[:, :whole]) + tiles_of(second[:, :whole]) + [ends]


def gather_tiles(tiles):
    packed = jnp.concatenate(tiles, axis=0)
    full = lax.all_gather(packed, FS, axis=0, tiled=True)
    return full.reshape(-1, len(tiles), SHARD, LANES)


def nt_dot(a, b):
    return lax.dot_general(a, b, (((1,), (1,)), ((), ())), preferred_element_type=jnp.float32)


def flat(ref, k):
    block = ref[:, k]
    return block.reshape(-1, LANES)


def ffn_kernel(rows_ref, first_ref, second_ref, down_ref, out_ref, hidden_ref):
    step = pl.program_id(0)
    last = pl.num_programs(0) - 1

    @pl.when(step < last)
    def _():
        both = jnp.concatenate([flat(first_ref, 0), flat(second_ref, 0)], axis=1)
        z = jnp.dot(rows_ref[...], both, preferred_element_type=jnp.float32)
        gate = z[:, :LANES]
        hidden = gate * jax.nn.sigmoid(gate) * z[:, LANES:]
        at = pl.multiple_of(step * LANES, LANES)
        hidden_ref[:, pl.ds(at, LANES)] = hidden.astype(jnp.bfloat16)

    @pl.when(step == last)
    def _():
        z = jnp.dot(rows_ref[...], flat(first_ref, 0), preferred_element_type=jnp.float32)
        hidden = z * jax.nn.sigmoid(z) * pltpu.roll(z, HALF, 1)
        lane = lax.broadcasted_iota(jnp.int32, z.shape, 1)
        hidden = jnp.where(lane < HALF, hidden, 0.0)
        tiles = hidden_ref.shape[1] // LANES
        hidden_ref[:, (tiles - 1) * LANES :] = hidden.astype(jnp.bfloat16)
        shards = 256 // SHARD
        for n in range(down_ref.shape[0] // shards):
            own = slice(n * shards, (n + 1) * shards)
            down = jnp.concatenate(
                [down_ref[own, k].reshape(-1, LANES) for k in range(tiles)], axis=1
            )
            out_ref[:, n * 256 : (n + 1) * 256] = nt_dot(hidden_ref[...], down).astype(
                jnp.bfloat16
            )


def ffn_terms(rows, packed):
    shards = packed.shape[0]
    length, width = rows.shape
    whole = lambda j: (0, 0)
    return pl.pallas_call(
        ffn_kernel,
        grid=(6,),
        in_specs=[
            pl.BlockSpec((length, width), whole),
            pl.BlockSpec((shards, 1, SHARD, LANES), lambda j: (0, jnp.where(j < 5, 6 + j, 16), 0, 0)),
            pl.BlockSpec((shards, 1, SHARD, LANES), lambda j: (0, jnp.minimum(11 + j, 15), 0, 0)),
            pl.BlockSpec((shards, 6, SHARD, LANES), lambda j: (0, 0, 0, 0)),
        ],
        out_specs=pl.BlockSpec((length, width), whole),
        out_shape=jax.ShapeDtypeStruct((length, width), jnp.bfloat16),
        scratch_shapes=[pltpu.VMEM((length, 6 * LANES), jnp.bfloat16)],
        compiler_params=pltpu.CompilerParams(vmem_limit_bytes=40 << 20),
        name="ffn",
    )(rows, packed, packed, packed)


def shifted(values, by, fill):
    row = lax.broadcasted_iota(jnp.int32, values.shape, 0)
    return jnp.where(row >= by, pltpu.roll(values, by, 0), fill)


def minus_expm1(x):
    series = 1.0 + x / 8.0
    for k in range(7, 1, -1):
        series = 1.0 + (x / k) * series
    return jnp.where(x > -0.5, -x * series, 1.0 - jnp.exp(x))


def scanned(keep, drive):
    by = 1
    while by < keep.shape[0]:
        drive = keep * shifted(drive, by, 0.0) + drive
        keep = keep * shifted(keep, by, 1.0)
        by *= 2
    return drive


def mixer_kernel(
    rows_ref, x_ref, gate_ref, ends_ref, out0_ref, out1_ref, taps_ref, a_ref, b_ref, rate_ref, out_ref
):
    rows = rows_ref[...]
    z = jnp.dot(
        rows, jnp.concatenate([flat(x_ref, 0), flat(gate_ref, 0)], axis=1), preferred_element_type=jnp.float32
    )
    ends = jnp.dot(rows, flat(ends_ref, 0), preferred_element_type=jnp.float32)
    lane = lax.broadcasted_iota(jnp.int32, ends.shape, 1)
    groups = (
        (z[:, :LANES], z[:, LANES:]),
        (jnp.where(lane < HALF, ends, 0.0), pltpu.roll(ends, HALF, 1)),
    )
    mixed = []
    for g, (lru_x, lru_gate) in enumerate(groups):
        lru_x = lru_x.astype(jnp.bfloat16).astype(jnp.float32)
        lru_gate = lru_gate.astype(jnp.bfloat16).astype(jnp.float32)
        own = slice(g * LANES, (g + 1) * LANES)
        taps = taps_ref[:, own]
        conv = taps[0:1] * lru_x
        for k in range(1, 4):
            conv = conv + taps[k : k + 1] * shifted(lru_x, k, 0.0)
        low = conv.astype(jnp.bfloat16)
        recall = jax.nn.sigmoid(jnp.dot(low, a_ref[g], preferred_element_type=jnp.float32))
        admit = jax.nn.sigmoid(jnp.dot(low, b_ref[g], preferred_element_type=jnp.float32))
        log_keep = recall * rate_ref[:, own]
        drive = jnp.sqrt(minus_expm1(2.0 * log_keep)) * admit * low.astype(jnp.float32)
        state = scanned(jnp.exp(log_keep), drive)
        mixed.append((state * jax.nn.gelu(lru_gate)).astype(jnp.bfloat16))
    shards = 256 // SHARD
    short = mixed[1][:, :HALF]
    for n in range(out0_ref.shape[0] // shards):
        own = slice(n * shards, (n + 1) * shards)
        terms = nt_dot(mixed[0], out0_ref[own, 0].reshape(-1, LANES))
        terms = terms + nt_dot(short, out1_ref[own, 0].reshape(-1, LANES)[:, HALF:])
        out_ref[:, n * 256 : (n + 1) * 256] = terms.astype(jnp.bfloat16)


def paired_blocks(blocks):
    zero = jnp.zeros_like(blocks[0])
    top = jnp.concatenate(
        [jnp.concatenate([blocks[0], zero], 1), jnp.concatenate([zero, blocks[1]], 1)], 0
    )
    end = jnp.concatenate(
        [jnp.concatenate([blocks[2], zero], 1), jnp.concatenate([zero, zero], 1)], 0
    )
    return jnp.stack([top, end])


def mixer_terms(rows, packed, conv_weight, gate_a_weight, gate_x_weight, decay_param):
    shards = packed.shape[0]
    length, width = rows.shape
    pad = ((0, 0), (0, HALF))
    taps = jnp.pad(conv_weight.astype(jnp.float32), pad)
    rate = jnp.pad(-8.0 * jax.nn.softplus(-decay_param)[None], pad)
    tile = lambda k: pl.BlockSpec((shards, 1, SHARD, LANES), lambda j: (0, k, 0, 0))
    whole = lambda *shape: pl.BlockSpec(shape, lambda j: (0,) * len(shape))
    return pl.pallas_call(
        mixer_kernel,
        grid=(1,),
        in_specs=[
            whole(length, width),
            tile(17),
            tile(18),
            tile(19),
            tile(20),
            tile(5),
            whole(4, 2 * LANES),
            whole(2, LANES, LANES),
            whole(2, LANES, LANES),
            whole(1, 2 * LANES),
        ],
        out_specs=whole(length, width),
        out_shape=jax.ShapeDtypeStruct((length, width), jnp.bfloat16),
        compiler_params=pltpu.CompilerParams(vmem_limit_bytes=40 << 20),
        name="mixer",
    )(
        rows,
        packed,
        packed,
        packed,
        packed,
        packed,
        taps,
        paired_blocks(gate_a_weight),
        paired_blocks(gate_x_weight),
        rate,
    )


def body(
    tokens,
    ffn1_gain,
    ffn1_gate,
    ffn1_up,
    ffn1_down,
    mix_gain,
    lru_in_weight,
    lru_gate_weight,
    conv_weight,
    gate_a_weight,
    gate_x_weight,
    decay_param,
    mix_out_weight,
    ffn2_gain,
    ffn2_gate,
    ffn2_up,
    ffn2_down,
):
    down = ffn1_down.T
    out = mix_out_weight.T
    packed1 = gather_tiles(
        tiles_of(down[:, :640])
        + [jnp.concatenate([down[:, 640:], out[:, LANES:]], axis=1)]
        + paired_tiles(ffn1_gate, ffn1_up)
        + paired_tiles(lru_in_weight, lru_gate_weight)
        + [out[:, :LANES]]
    )
    down = ffn2_down.T
    packed2 = gather_tiles(
        tiles_of(down[:, :640])
        + [jnp.pad(down[:, 640:], ((0, 0), (0, HALF)))]
        + paired_tiles(ffn2_gate, ffn2_up)
    )
    rows = gather_rows(rms_rows(tokens, ffn1_gain))
    terms = ffn_terms(rows, packed1)
    first = (tokens.astype(jnp.float32) + 0.5 * reduce_rows(terms)).astype(jnp.bfloat16)
    rows = gather_rows(rms_rows(first, mix_gain))
    terms = mixer_terms(rows, packed1, conv_weight, gate_a_weight, gate_x_weight, decay_param)
    second = (first.astype(jnp.float32) + reduce_rows(terms)).astype(jnp.bfloat16)
    rows = gather_rows(rms_rows(second, ffn2_gain))
    terms = ffn_terms(rows, packed2)
    return (second.astype(jnp.float32) + 0.5 * reduce_rows(terms)).astype(jnp.bfloat16)


def solution(mesh):
    split = Mesh(mesh.devices.reshape(8, 4, mesh.shape["tp"]), ("fs_0", "fs_1", "tp"))
    placed = (
        P(FS_TP, None),
        P(),
        P(FS, "tp"),
        P(FS, "tp"),
        P("tp", FS),
        P(),
        P(FS, "tp"),
        P(FS, "tp"),
        P(None, "tp"),
        P("tp", None, None),
        P("tp", None, None),
        P("tp"),
        P("tp", FS),
        P(),
        P(FS, "tp"),
        P(FS, "tp"),
        P("tp", FS),
    )
    return jax.shard_map(
        body, mesh=split, in_specs=placed, out_specs=P(FS_TP, None), check_vma=False
    )
```

time: 397 us -> 306 us (0.77)
  waiting for transfers between devices: 182 us -> 123 us
  blocking collectives: 130 us -> 100 us
  matrix products: 29.7 us -> 0 us
  local copies, waits for them, and re-layouts: 13.1 us -> 38.8 us
  Pallas kernels: 0 us -> 15.6 us
  other arithmetic: 10.3 us -> 2.84 us
  starting transfers between devices: 16.6 us -> 9.21 us
    all_gather x5 -> x2, waiting for transfers between devices: 166 us -> 82.3 us  [gather_tiles(): full = lax.all_gather(packed, FS, axis=0, tiled=True)]
    dot_general x8 -> x0, matrix products: 29.7 us -> none  [the longest x2 16.5 us: block_terms(): jnp.dot(hidden, gathered_by_axis(down_weight, FS, 1), preferred_element_t...]
    unnamed x24 -> x63, local copies, waits for them, and re-layouts: 0.6 us -> 30.1 us
    all_to_all x3 -> x2, waiting for transfers between devices: 16.1 us -> 40.9 us  [gather_rows(): lax.all_to_all(copies, 'tp', split_axis=0, concat_axis=0, tiled=True)]
    all_gather x2 -> x0, blocking collectives: 24.3 us -> none  [gathered_by_axis(): value = lax.all_gather(value, axis, axis=dim, tiled=True)]
    pallas_call x0 -> x3, Pallas kernels: none -> 15.6 us  [the longest x2 12 us: ffn_terms(): pl.pallas_call(ffn_kernel, grid=(6,), in_specs=[pl.BlockSpec((length, wid...]
    all_to_all x3 -> x2, starting transfers between devices: 16.4 us -> 9.13 us  [gather_rows(): lax.all_to_all(copies, 'tp', split_axis=0, concat_axis=0, tiled=True)]
    all_to_all x4, blocking collectives: 106 us -> 100 us  [the longest x3 73.9 us: reduce_rows(): lax.all_to_all(blocks, 'tp', split_axis=0, concat_axis=0, tiled=True)]
  transfers between devices with their start and end apart: 8 -> 4, of which waited for: 7 -> 3; matrix products, arithmetic and copies ran while one was open for 10% -> 3% of each run, Pallas kernels for 0% -> 3%
where the time goes in v1:
time: 306 us; the launch traced here: 303 us
  waiting for transfers between devices  123 us (40%)
  blocking collectives  100 us (33%)
  local copies, waits for them, and re-layouts  38.8 us (13%)
  Pallas kernels  15.6 us (5%)
  between operations  13.7 us (4%)
  starting transfers between devices  9.21 us (3%)
    all_gather x2, waiting for transfers between devices, gather_tiles(): full = lax.all_gather(packed, FS, axis=0, tiled=True)  82.3 us
    all_to_all x3, blocking collectives, reduce_rows(): lax.all_to_all(blocks, 'tp', split_axis=0, concat_axis=0, tiled=True)  73.9 us
    all_to_all x2, waiting for transfers between devices, gather_rows(): lax.all_to_all(copies, 'tp', split_axis=0, concat_axis=0, tiled=True)  40.9 us
    unnamed x63, local copies, waits for them, and re-layouts  30.1 us
    all_to_all x1, blocking collectives, gather_rows(): lax.all_to_all(copies, 'tp', split_axis=0, concat_axis=0, tiled=True)  26.2 us
    pallas_call x2, Pallas kernels, ffn_terms(): pl.pallas_call(ffn_kernel, grid=(6,), in_specs=[pl.BlockSpec((length, wid...  12 us
    all_to_all x2, starting transfers between devices, gather_rows(): lax.all_to_all(copies, 'tp', split_axis=0, concat_axis=0, tiled=True)  9.13 us
  transfers between devices with their start and end apart: 4, of which 3 were waited for; matrix products, arithmetic and copies ran while one was open for 3% of the time, Pallas kernels for 3%

profile of v1, /device:TPU:1, one launch (start us, length us, event | category | flops | bytes accessed | tf_op | source)
XLA Modules:
  0.0 303.5 jit_solution(3333607471616326320)
XLA Ops:
  6.6 0.8 constant_dynamic-update-slice_fusion.20
  10.3 0.7 constant_dynamic-update-slice_fusion.16
  12.5 0.7 constant_dynamic-update-slice_fusion.14
  16.9 0.7 constant_dynamic-update-slice_fusion.9
  21.3 0.7 constant_dynamic-update-slice_fusion.3
  23.6 0.7 constant_dynamic-update-slice_fusion
  30.9 26.2 %all_to_all.30 = bf16[8,48,2048]{2,1,0:T(8,128)(2,1)S(1)} all-to-all(bf16[8,48,2048]{2,1,0:T(8,128)(2,1)S(1)} %broadcast_in_dim.6), channel_id=1, replica_groups=mesh['fs_0'=8,'fs_1'=4,'tp'=8] {'tp'}, dimensions={0} | all-to-all | bytes 3145728 | tf_op jit(solution)/shard_map/all_to_all | solution.py:26
  57.1 82.3 %all-gather.3.cloned.1.call-done = bf16[43008,128]{1,0:T(8,128)(2,1)} async-done(((bf16[1344,128]{1,0:T(8,128)(2,1)}), bf16[43008,128]{1,0:T(8,128)(2,1)}) %all-gather.3.cloned.1.call-update) | async-done | bytes 11010064 | tf_op jit(solution)/shard_map/all_gather | solution.py:48
  139.4 4.1 %copy-done = bf16[43008,128]{1,0:T(8,128)(2,1)S(1)} copy-done((bf16[43008,128]{1,0:T(8,128)(2,1)S(1)}, bf16[43008,128]{1,0:T(8,128)(2,1)}, u32[]{:S(2)}) %copy-start) | copy-done | bytes 11010072
  143.5 6.0 %ffn.2 = bf16[384,2048]{1,0:T(8,128)(2,1)S(1)} custom-call(bf16[384,2048]{1,0:T(8,128)(2,1)S(1)} %bitcast.44, bf16[32,21,64,128]{3,2,1,0:T(8,128)(2,1)S(1)} %bitcast.32, bf16[32,21,64,128]{3,2,1,0:T(8,128)(2,1)S(1)} %bitcast.33, bf16[32,21,64,128]{3,2,1,0:T(8,128)(2,1)S(1)} %bitcast.34), custom_call_target="tpu_custom_call" | custom-call | tf_op jit(solution)/shard_map/ffn/pallas_call | solution.py:97
  149.5 26.1 %all_to_all.31 = bf16[8,48,2048]{2,1,0:T(8,128)(2,1)S(1)} all-to-all(bf16[8,48,2048]{2,1,0:T(8,128)(2,1)S(1)} %bitcast.46), channel_id=1, replica_groups=mesh['fs_0'=8,'fs_1'=4,'tp'=8] {'tp'}, dimensions={0} | all-to-all | bytes 3145728 | tf_op jit(solution)/shard_map/all_to_all | solution.py:32
  176.4 1.3 broadcast_in_dim.7
  177.8 4.6 %all-to-all-start.2 = ((bf16[8,48,2048]{2,1,0:T(8,128)(2,1)}), bf16[8,48,2048]{2,1,0:T(8,128)(2,1)S(1)}, u32[]{:S(2)}, u32[]{:S(2)}) async-start(bf16[8,48,2048]{2,1,0:T(8,128)(2,1)} %broadcast_in_dim.7), calls=%async_computation.2 | async-start | bytes 3145728 | tf_op jit(solution)/shard_map/all_to_all | solution.py:26
  182.6 20.3 %all-to-all-done.2 = bf16[8,48,2048]{2,1,0:T(8,128)(2,1)S(1)} async-done(((bf16[8,48,2048]{2,1,0:T(8,128)(2,1)}), bf16[8,48,2048]{2,1,0:T(8,128)(2,1)S(1)}, u32[]{:S(2)}, u32[]{:S(2)}) %all-to-all-start.2) | async-done | bytes 1572896 | tf_op jit(solution)/shard_map/all_to_all | solution.py:26
  203.0 4.4 %copy-done.1 = bf16[43008,128]{1,0:T(8,128)(2,1)S(1)} copy-done((bf16[43008,128]{1,0:T(8,128)(2,1)S(1)}, bf16[43008,128]{1,0:T(8,128)(2,1)}, u32[]{:S(2)}) %copy-start.1) | copy-done | bytes 11010072
  207.4 3.6 %mixer.1 = bf16[384,2048]{1,0:T(8,128)(2,1)S(1)} custom-call(bf16[384,2048]{1,0:T(8,128)(2,1)S(1)} %bitcast.47, bf16[32,21,64,128]{3,2,1,0:T(8,128)(2,1)S(1)} %bitcast.35, bf16[32,21,64,128]{3,2,1,0:T(8,128)(2,1)S(1)} %bitcast.36, bf16[32,21,64,128]{3,2,1,0:T(8,128)(2,1)S(1)} %bitcast.37, bf16[32,21,64,128]{3,2,1,0:T(8,128)(2,1)S(1)} %bitcast.38, ...), custom_call_target="tpu_custom_call" | custom-call | tf_op jit(solution)/shard_map/mixer/pallas_call | solution.py:192
  211.0 23.9 %all_to_all.32 = bf16[8,48,2048]{2,1,0:T(8,128)(2,1)S(1)} all-to-all(bf16[8,48,2048]{2,1,0:T(8,128)(2,1)S(1)} %bitcast.48), channel_id=1, replica_groups=mesh['fs_0'=8,'fs_1'=4,'tp'=8] {'tp'}, dimensions={0} | all-to-all | bytes 3145728 | tf_op jit(solution)/shard_map/all_to_all | solution.py:32
  235.7 1.4 broadcast_in_dim.8
  237.1 4.5 %all-to-all-start.4 = ((bf16[8,48,2048]{2,1,0:T(8,128)(2,1)}), bf16[8,48,2048]{2,1,0:T(8,128)(2,1)S(1)}, u32[]{:S(2)}, u32[]{:S(2)}) async-start(bf16[8,48,2048]{2,1,0:T(8,128)(2,1)} %broadcast_in_dim.8), calls=%async_computation.4 | async-start | bytes 3145728 | tf_op jit(solution)/shard_map/all_to_all | solution.py:26
  241.6 20.6 %all-to-all-done.4 = bf16[8,48,2048]{2,1,0:T(8,128)(2,1)S(1)} async-done(((bf16[8,48,2048]{2,1,0:T(8,128)(2,1)}), bf16[8,48,2048]{2,1,0:T(8,128)(2,1)S(1)}, u32[]{:S(2)}, u32[]{:S(2)}) %all-to-all-start.4) | async-done | bytes 1572896 | tf_op jit(solution)/shard_map/all_to_all | solution.py:26
  262.2 3.5 %copy-done.2 = bf16[34816,128]{1,0:T(8,128)(2,1)S(1)} copy-done((bf16[34816,128]{1,0:T(8,128)(2,1)S(1)}, bf16[34816,128]{1,0:T(8,128)(2,1)}, u32[]{:S(2)}) %copy-start.2) | copy-done | bytes 8912920
  265.7 6.0 %ffn.3 = bf16[384,2048]{1,0:T(8,128)(2,1)S(1)} custom-call(bf16[384,2048]{1,0:T(8,128)(2,1)S(1)} %bitcast.43, bf16[32,17,64,128]{3,2,1,0:T(8,128)(2,1)S(1)} %bitcast.40, bf16[32,17,64,128]{3,2,1,0:T(8,128)(2,1)S(1)} %bitcast.41, bf16[32,17,64,128]{3,2,1,0:T(8,128)(2,1)S(1)} %bitcast.42), custom_call_target="tpu_custom_call" | custom-call | tf_op jit(solution)/shard_map/ffn/pallas_call | solution.py:97
  271.7 23.9 %all_to_all.33 = bf16[8,48,2048]{2,1,0:T(8,128)(2,1)S(1)} all-to-all(bf16[8,48,2048]{2,1,0:T(8,128)(2,1)S(1)} %bitcast.45), channel_id=1, replica_groups=mesh['fs_0'=8,'fs_1'=4,'tp'=8] {'tp'}, dimensions={0} | all-to-all | bytes 3145728 | tf_op jit(solution)/shard_map/all_to_all | solution.py:32
  295.9 0.7 fusion.11
  (97 shorter events, 21.9 us)
Async XLA Ops:
  6.5 22.9 %copy-start.6 = (bf16[64,704]{1,0:T(8,128)(2,1)S(1)}, bf16[64,704]{1,0:T(8,128)(2,1)}, u32[]{:S(2)}) copy-start(bf16[64,704]{1,0:T(8,128)(2,1)} %param.31) | copy-start | bytes 270340
  6.5 23.1 %slice-start = ((bf16[64,704]{1,0:T(8,128)(2,1)}), bf16[64,64]{1,0:T(8,128)(2,1)S(1)}, s32[]{:S(2)}) async-start(bf16[64,704]{1,0:T(8,128)(2,1)} %param.31), calls=%async_computation.8 | async-start | bytes 32768 | tf_op jit(solution)/shard_map/slice | solution.py:42
  6.5 23.0 %copy-start.7 = (bf16[64,704]{1,0:T(8,128)(2,1)S(1)}, bf16[64,704]{1,0:T(8,128)(2,1)}, u32[]{:S(2)}) copy-start(bf16[64,704]{1,0:T(8,128)(2,1)} %param.32) | copy-start | bytes 270340
  6.5 23.1 %slice-start.1 = ((bf16[64,704]{1,0:T(8,128)(2,1)}), bf16[64,64]{1,0:T(8,128)(2,1)S(1)}, s32[]{:S(2)}) async-start(bf16[64,704]{1,0:T(8,128)(2,1)} %param.32), calls=%async_computation.9 | async-start | bytes 32768 | tf_op jit(solution)/shard_map/slice | solution.py:42
  6.5 23.9 %copy-start.3 = (bf16[48,2048]{1,0:T(8,128)(2,1)S(1)}, bf16[48,2048]{1,0:T(8,128)(2,1)}, u32[]{:S(2)}) copy-start(bf16[48,2048]{1,0:T(8,128)(2,1)} %param.17) | copy-start | bytes 589828
  6.5 24.1 %copy-start.10 = (f32[2048]{0:T(1024)S(1)}, f32[2048]{0:T(1024)}, u32[]{:S(2)}) copy-start(f32[2048]{0:T(1024)} %param.18) | copy-start | bytes 24580
  6.6 132.8 %all-gather.3.cloned.1.call-start = ((), (), s32[]{:S(2)}) async-start(), calls=%async_computation.6 | async-start | bytes 11354112 | tf_op jit(solution)/shard_map/all_gather | solution.py:48
  24.3 0.7 copy-start.4
  25.0 216.6 %all-gather.5.cloned.1.call-start = ((), (), s32[]{:S(2)}) async-start(), calls=%async_computation.7 | async-start | bytes 9191424 | tf_op jit(solution)/shard_map/all_gather | solution.py:48
  29.7 0.7 copy-start.5
  139.4 4.1 %copy-start = (bf16[43008,128]{1,0:T(8,128)(2,1)S(1)}, bf16[43008,128]{1,0:T(8,128)(2,1)}, u32[]{:S(2)}) copy-start(bf16[43008,128]{1,0:T(8,128)(2,1)} %all-gather.3.cloned.1.call-done) | copy-start | bytes 33030148
  175.6 0.7 copy-start.11
  177.7 4.6 %copy-start.14 = (f32[192]{0:T(256)S(1)}, f32[192]{0:T(256)}, u32[]{:S(2)}) copy-start(f32[192]{0:T(256)} %param.28) | copy-start | bytes 2308
  177.7 4.7 %copy-start.13 = (bf16[4,192]{1,0:T(4,128)(2,1)S(1)}, bf16[4,192]{1,0:T(4,128)(2,1)}, u32[]{:S(2)}) copy-start(bf16[4,192]{1,0:T(4,128)(2,1)} %param.25) | copy-start | bytes 4612
  177.7 4.7 %copy-start.8 = (bf16[3,64,64]{2,1,0:T(8,128)(2,1)S(1)}, bf16[3,64,64]{2,1,0:T(8,128)(2,1)}, u32[]{:S(2)}) copy-start(bf16[3,64,64]{2,1,0:T(8,128)(2,1)} %param.26) | copy-start | bytes 73732
  177.8 4.8 %copy-start.9 = (bf16[3,64,64]{2,1,0:T(8,128)(2,1)S(1)}, bf16[3,64,64]{2,1,0:T(8,128)(2,1)}, u32[]{:S(2)}) copy-start(bf16[3,64,64]{2,1,0:T(8,128)(2,1)} %param.27) | copy-start | bytes 73732
  177.8 25.2 %all-to-all-start.2 = ((bf16[8,48,2048]{2,1,0:T(8,128)(2,1)}), bf16[8,48,2048]{2,1,0:T(8,128)(2,1)S(1)}, u32[]{:S(2)}, u32[]{:S(2)}) async-start(bf16[8,48,2048]{2,1,0:T(8,128)(2,1)} %broadcast_in_dim.7), calls=%async_computation.2 | async-start | bytes 3145728 | tf_op jit(solution)/shard_map/all_to_all | solution.py:26
  203.0 4.4 %copy-start.1 = (bf16[43008,128]{1,0:T(8,128)(2,1)S(1)}, bf16[43008,128]{1,0:T(8,128)(2,1)}, u32[]{:S(2)}) copy-start(bf16[43008,128]{1,0:T(8,128)(2,1)} %all-gather.3.cloned.1.call-done) | copy-start | bytes 33030148
  234.9 0.7 copy-start.12
  237.1 25.1 %all-to-all-start.4 = ((bf16[8,48,2048]{2,1,0:T(8,128)(2,1)}), bf16[8,48,2048]{2,1,0:T(8,128)(2,1)S(1)}, u32[]{:S(2)}, u32[]{:S(2)}) async-start(bf16[8,48,2048]{2,1,0:T(8,128)(2,1)} %broadcast_in_dim.8), calls=%async_computation.4 | async-start | bytes 3145728 | tf_op jit(solution)/shard_map/all_to_all | solution.py:26
  262.2 3.5 %copy-start.2 = (bf16[34816,128]{1,0:T(8,128)(2,1)S(1)}, bf16[34816,128]{1,0:T(8,128)(2,1)}, u32[]{:S(2)}) copy-start(bf16[34816,128]{1,0:T(8,128)(2,1)} %all-gather.5.cloned.1.call-done) | copy-start | bytes 26738692
Sparse Core Ops, SparseCore 0:
  25.2 114.1 all-gather.2
  142.0 97.5 all-gather.4

commit v2 on v1

v2 whole, which is shorter than its diff:
```python
import jax
import jax.numpy as jnp
from jax import lax
from jax.experimental import pallas as pl
from jax.experimental.pallas import tpu as pltpu
from jax.sharding import Mesh
from jax.sharding import PartitionSpec as P

FS = ("z", "y")
TP = ("x", "c")
FS_TP = ("z", "y", "x", "c")

EPS = 1e-06
LANES = 128
SHARD = 64
HALF = 64


def moved(value, axis, by):
    count = lax.axis_size(axis)
    return lax.ppermute(value, axis, [(i, (i - by) % count) for i in range(count)])


def in_hbm(value):
    return pltpu.with_memory_space_constraint(value, pltpu.HBM)


def whole(*shape):
    return pl.BlockSpec(shape, lambda *_: (0,) * len(shape))


def norm_of(wide, gain):
    scale = lax.rsqrt(jnp.mean(wide * wide, axis=-1, keepdims=True) + EPS)
    return (wide * scale * gain).astype(jnp.bfloat16)


def norm_kernel(rows_ref, gain_ref, out_ref):
    out_ref[...] = norm_of(rows_ref[...].astype(jnp.float32), gain_ref[...])


def rms_rows(values, gain):
    return pl.pallas_call(
        norm_kernel,
        out_shape=jax.ShapeDtypeStruct(values.shape, jnp.bfloat16),
        name="norm",
    )(values, gain[None])


def gather_rows(own):
    near = moved(own, "x", 1)
    far = moved(own, "x", 3)
    across = moved(own, "x", 2)
    mine = jnp.concatenate([own, near, across, far], axis=0)
    return mine, moved(mine, "c", 1)


def pair_sum_kernel(mine_ref, other_ref, *out_refs):
    rows = out_refs[0].shape[0]
    for n, out_ref in enumerate(out_refs):
        own = slice(n * rows, (n + 1) * rows)
        out_ref[...] = (
            mine_ref[own].astype(jnp.float32) + other_ref[own].astype(jnp.float32)
        ).astype(jnp.bfloat16)


def sent_sums(terms):
    mine, other = terms
    other = moved(other, "c", 1)
    count = lax.axis_size("x")
    shape = jax.ShapeDtypeStruct((mine.shape[0] // count, mine.shape[1]), jnp.bfloat16)
    sums = pl.pallas_call(pair_sum_kernel, out_shape=[shape] * count, name="pair_sum")(mine, other)
    return [sums[0]] + [moved(sums[n], "x", -n) for n in range(1, count)]


def combine_kernel(half, base_ref, a_ref, b_ref, c_ref, d_ref, *refs):
    total = a_ref[...].astype(jnp.float32) + b_ref[...].astype(jnp.float32)
    total = total + c_ref[...].astype(jnp.float32) + d_ref[...].astype(jnp.float32)
    if half:
        total = 0.5 * total
    result = (base_ref[...].astype(jnp.float32) + total).astype(jnp.bfloat16)
    if len(refs) == 1:
        refs[0][...] = result
    else:
        gain_ref, out_ref, norm_ref = refs
        out_ref[...] = result
        norm_ref[...] = norm_of(result.astype(jnp.float32), gain_ref[...])


def combined(base, sums, half, gain=None):
    shape = jax.ShapeDtypeStruct(base.shape, jnp.bfloat16)
    extra = () if gain is None else (gain[None],)
    outs = [shape] if gain is None else [shape, shape]
    return pl.pallas_call(
        lambda *refs: combine_kernel(half, *refs), out_shape=outs, name="combine"
    )(base, *sums, *extra)


def pack_kernel(plan, *refs):
    *in_refs, out_ref = refs
    for n, parts in enumerate(plan):
        pieces = [in_refs[which][:, at : at + size] for which, at, size in parts]
        if len(pieces) == 2:
            low, high = (p.astype(jnp.float32) for p in pieces)
            tile = jnp.concatenate([low, high], axis=1).astype(jnp.bfloat16)
        else:
            tile = pieces[0]
        if tile.shape[1] < LANES:
            out_ref[n * SHARD : (n + 1) * SHARD] = jnp.zeros((SHARD, LANES), jnp.bfloat16)
        out_ref[n * SHARD : (n + 1) * SHARD, : tile.shape[1]] = tile


def packed_tiles(plan, arrays):
    return pl.pallas_call(
        lambda *refs: pack_kernel(plan, *refs),
        out_shape=jax.ShapeDtypeStruct((len(plan) * SHARD, LANES), jnp.bfloat16),
        name="pack",
    )(*arrays)


def full_tiles(which, count):
    return [((which, k * LANES, LANES),) for k in range(count)]


def gather_tiles(plan, arrays):
    packed = packed_tiles(plan, arrays)
    full = lax.all_gather(packed, FS, axis=0, tiled=True)
    return in_hbm(full.reshape(-1, len(plan), SHARD, LANES))


def nt_dot(a, b):
    return lax.dot_general(a, b, (((1,), (1,)), ((), ())), preferred_element_type=jnp.float32)


def flat(ref, k):
    block = ref[:, k]
    return block.reshape(-1, LANES)


def ffn_kernel(
    mine_ref, other_ref, first_ref, second_ref, down_ref, out_mine_ref, out_other_ref, hidden_ref, rows_ref
):
    step = pl.program_id(0)
    last = pl.num_programs(0) - 1
    half = mine_ref.shape[0]

    @pl.when(step == 0)
    def _():
        rows_ref[:half] = mine_ref[...]
        rows_ref[half:] = other_ref[...]

    @pl.when(step < last)
    def _():
        both = jnp.concatenate([flat(first_ref, 0), flat(second_ref, 0)], axis=1)
        z = jnp.dot(rows_ref[...], both, preferred_element_type=jnp.float32)
        gate = z[:, :LANES]
        hidden = gate * jax.nn.sigmoid(gate) * z[:, LANES:]
        at = pl.multiple_of(step * LANES, LANES)
        hidden_ref[:, pl.ds(at, LANES)] = hidden.astype(jnp.bfloat16)

    @pl.when(step == last)
    def _():
        z = jnp.dot(rows_ref[...], flat(first_ref, 0), preferred_element_type=jnp.float32)
        hidden = z * jax.nn.sigmoid(z) * pltpu.roll(z, HALF, 1)
        lane = lax.broadcasted_iota(jnp.int32, z.shape, 1)
        hidden = jnp.where(lane < HALF, hidden, 0.0)
        tiles = hidden_ref.shape[1] // LANES
        hidden_ref[:, (tiles - 1) * LANES :] = hidden.astype(jnp.bfloat16)
        shards = 256 // SHARD
        for n in range(down_ref.shape[0] // shards):
            own = slice(n * shards, (n + 1) * shards)
            down = jnp.concatenate(
                [down_ref[own, k].reshape(-1, LANES) for k in range(tiles)], axis=1
            )
            terms = nt_dot(hidden_ref[...], down).astype(jnp.bfloat16)
            out_mine_ref[:, n * 256 : (n + 1) * 256] = terms[:half]
            out_other_ref[:, n * 256 : (n + 1) * 256] = terms[half:]


def ffn_terms(rows, packed):
    shards = packed.shape[0]
    half, width = rows[0].shape
    return pl.pallas_call(
        ffn_kernel,
        grid=(6,),
        in_specs=[
            whole(half, width),
            whole(half, width),
            pl.BlockSpec((shards, 1, SHARD, LANES), lambda j: (0, jnp.where(j < 5, 6 + j, 16), 0, 0)),
            pl.BlockSpec((shards, 1, SHARD, LANES), lambda j: (0, jnp.minimum(11 + j, 15), 0, 0)),
            pl.BlockSpec((shards, 6, SHARD, LANES), lambda j: (0, 0, 0, 0)),
        ],
        out_specs=[whole(half, width)] * 2,
        out_shape=[jax.ShapeDtypeStruct((half, width), jnp.bfloat16)] * 2,
        scratch_shapes=[
            pltpu.VMEM((2 * half, 6 * LANES), jnp.bfloat16),
            pltpu.VMEM((2 * half, width), jnp.bfloat16),
        ],
        compiler_params=pltpu.CompilerParams(vmem_limit_bytes=40 << 20),
        name="ffn",
    )(*rows, packed, packed, packed)


def shifted(values, by, fill):
    row = lax.broadcasted_iota(jnp.int32, values.shape, 0)
    return jnp.where(row >= by, pltpu.roll(values, by, 0), fill)


def minus_expm1(x):
    series = 1.0 + x / 8.0
    for k in range(7, 1, -1):
        series = 1.0 + (x / k) * series
    return jnp.where(x > -0.5, -x * series, 1.0 - jnp.exp(x))


def scanned(keep, drive):
    by = 1
    while by < keep.shape[0]:
        drive = keep * shifted(drive, by, 0.0) + drive
        keep = keep * shifted(keep, by, 1.0)
        by *= 2
    return drive


def mixer_kernel(
    mine_ref,
    other_ref,
    x_ref,
    gate_ref,
    ends_ref,
    out0_ref,
    out1_ref,
    taps_ref,
    a_ref,
    b_ref,
    rate_ref,
    out_mine_ref,
    out_other_ref,
    order_ref,
):
    half = mine_ref.shape[0]
    chips = lax.axis_size("x")
    block = half // chips
    x = lax.axis_index("x")
    core = lax.axis_index("c")
    weights = jnp.concatenate([flat(x_ref, 0), flat(gate_ref, 0), flat(ends_ref, 0)], axis=1)
    places = []
    for n, ref in enumerate((mine_ref, other_ref)):
        part = jnp.dot(ref[...], weights, preferred_element_type=jnp.float32)
        for k in range(chips):
            chip = lax.rem(x + k, chips)
            which = core if n == 0 else 1 - core
            place = pl.multiple_of((chip * 2 + which) * block, block)
            places.append(place)
            order_ref[pl.ds(place, block), :] = part[k * block : (k + 1) * block]
    z = order_ref[:, : 2 * LANES]
    ends = order_ref[:, 2 * LANES :]
    lane = lax.broadcasted_iota(jnp.int32, ends.shape, 1)
    groups = (
        (z[:, :LANES], z[:, LANES:]),
        (jnp.where(lane < HALF, ends, 0.0), pltpu.roll(ends, HALF, 1)),
    )
    mixed = []
    for g, (lru_x, lru_gate) in enumerate(groups):
        lru_x = lru_x.astype(jnp.bfloat16).astype(jnp.float32)
        lru_gate = lru_gate.astype(jnp.bfloat16).astype(jnp.float32)
        own = slice(g * LANES, (g + 1) * LANES)
        taps = taps_ref[:, own]
        conv = taps[0:1] * lru_x
        for k in range(1, 4):
            conv = conv + taps[k : k + 1] * shifted(lru_x, k, 0.0)
        low = conv.astype(jnp.bfloat16)
        recall = jax.nn.sigmoid(jnp.dot(low, a_ref[g], preferred_element_type=jnp.float32))
        admit = jax.nn.sigmoid(jnp.dot(low, b_ref[g], preferred_element_type=jnp.float32))
        log_keep = recall * rate_ref[:, own]
        drive = jnp.sqrt(minus_expm1(2.0 * log_keep)) * admit * low.astype(jnp.float32)
        state = scanned(jnp.exp(log_keep), drive)
        mixed.append(state * jax.nn.gelu(lru_gate))
    for g in range(2):
        order_ref[:, g * LANES : (g + 1) * LANES] = mixed[g]
    mixed = jnp.concatenate([order_ref[pl.ds(p, block), : 2 * LANES] for p in places], axis=0)
    mixed = mixed.astype(jnp.bfloat16)
    full = mixed[:, :LANES]
    short = mixed[:, LANES : LANES + HALF]
    shards = 256 // SHARD
    for n in range(out0_ref.shape[0] // shards):
        own = slice(n * shards, (n + 1) * shards)
        terms = nt_dot(full, out0_ref[own, 0].reshape(-1, LANES))
        terms = terms + nt_dot(short, out1_ref[own, 0].reshape(-1, LANES)[:, HALF:])
        terms = terms.astype(jnp.bfloat16)
        out_mine_ref[:, n * 256 : (n + 1) * 256] = terms[:half]
        out_other_ref[:, n * 256 : (n + 1) * 256] = terms[half:]


def paired_blocks(blocks):
    zero = jnp.zeros_like(blocks[0])
    top = jnp.concatenate(
        [jnp.concatenate([blocks[0], zero], 1), jnp.concatenate([zero, blocks[1]], 1)], 0
    )
    end = jnp.concatenate(
        [jnp.concatenate([blocks[2], zero], 1), jnp.concatenate([zero, zero], 1)], 0
    )
    return jnp.stack([top, end])


def mixer_terms(rows, packed, conv_weight, gate_a_weight, gate_x_weight, decay_param):
    shards = packed.shape[0]
    half, width = rows[0].shape
    pad = ((0, 0), (0, HALF))
    taps = jnp.pad(conv_weight.astype(jnp.float32), pad)
    rate = jnp.pad(-8.0 * jax.nn.softplus(-decay_param)[None], pad)
    tile = lambda k: pl.BlockSpec((shards, 1, SHARD, LANES), lambda j: (0, k, 0, 0))
    return pl.pallas_call(
        mixer_kernel,
        grid=(1,),
        in_specs=[
            whole(half, width),
            whole(half, width),
            tile(17),
            tile(18),
            tile(19),
            tile(20),
            tile(5),
            whole(4, 2 * LANES),
            whole(2, LANES, LANES),
            whole(2, LANES, LANES),
            whole(1, 2 * LANES),
        ],
        out_specs=[whole(half, width)] * 2,
        out_shape=[jax.ShapeDtypeStruct((half, width), jnp.bfloat16)] * 2,
        scratch_shapes=[pltpu.VMEM((2 * half, 3 * LANES), jnp.float32)],
        compiler_params=pltpu.CompilerParams(vmem_limit_bytes=40 << 20),
        name="mixer",
    )(
        *rows,
        packed,
        packed,
        packed,
        packed,
        packed,
        taps,
        paired_blocks(gate_a_weight),
        paired_blocks(gate_x_weight),
        rate,
    )


def body(
    tokens,
    ffn1_gain,
    ffn1_gate,
    ffn1_up,
    ffn1_down,
    mix_gain,
    lru_in_weight,
    lru_gate_weight,
    conv_weight,
    gate_a_weight,
    gate_x_weight,
    decay_param,
    mix_out_weight,
    ffn2_gain,
    ffn2_gate,
    ffn2_up,
    ffn2_down,
):
    plan = full_tiles(0, 5) + [((0, 640, HALF), (1, LANES, HALF))]
    plan += full_tiles(2, 5) + full_tiles(3, 5) + [((2, 640, HALF), (3, 640, HALF))]
    plan += full_tiles(4, 1) + full_tiles(5, 1) + [((4, LANES, HALF), (5, LANES, HALF))]
    plan += full_tiles(1, 1)
    packed1 = gather_tiles(
        plan, [ffn1_down.T, mix_out_weight.T, ffn1_gate, ffn1_up, lru_in_weight, lru_gate_weight]
    )
    plan = full_tiles(0, 5) + [((0, 640, HALF),)]
    plan += full_tiles(1, 5) + full_tiles(2, 5) + [((1, 640, HALF), (2, 640, HALF))]
    packed2 = gather_tiles(plan, [ffn2_down.T, ffn2_gate, ffn2_up])
    rows = gather_rows(rms_rows(tokens, ffn1_gain))
    sums = sent_sums(ffn_terms(rows, packed1))
    first, normed = combined(tokens, sums, True, mix_gain)
    rows = gather_rows(normed)
    sums = sent_sums(
        mixer_terms(rows, packed1, conv_weight, gate_a_weight, gate_x_weight, decay_param)
    )
    second, normed = combined(first, sums, False, ffn2_gain)
    rows = gather_rows(normed)
    sums = sent_sums(ffn_terms(rows, packed2))
    return combined(second, sums, True)[0]


def solution(mesh):
    split = Mesh(mesh.devices.reshape(8, 4, 4, 2), FS_TP)
    placed = (
        P(FS_TP, None),
        P(),
        P(FS, TP),
        P(FS, TP),
        P(TP, FS),
        P(),
        P(FS, TP),
        P(FS, TP),
        P(None, TP),
        P(TP, None, None),
        P(TP, None, None),
        P(TP),
        P(TP, FS),
        P(),
        P(FS, TP),
        P(FS, TP),
        P(TP, FS),
    )
    return jax.shard_map(
        body, mesh=split, in_specs=placed, out_specs=P(FS_TP, None), check_vma=False
    )
```

time: 306 us -> 264 us (0.86)
  blocking collectives: 100 us -> 0 us
  waiting for transfers between devices: 123 us -> 166 us
  local copies, waits for them, and re-layouts: 38.8 us -> 9.6 us
  Pallas kernels: 15.6 us -> 42.4 us
  starting transfers between devices: 9.21 us -> 30.3 us
    all_to_all x4 -> x0, blocking collectives: 100 us -> none  [the longest x3 73.9 us: reduce_rows(): lax.all_to_all(blocks, 'tp', split_axis=0, concat_axis=0, tiled=True)]
    ppermute x0 -> x24, waiting for transfers between devices: none -> 64.6 us  [moved(): lax.ppermute(value, axis, [(i, (i - by) % count) for i in range(count)])]
    all_to_all x2 -> x0, waiting for transfers between devices: 40.9 us -> none  [gather_rows(): lax.all_to_all(copies, 'tp', split_axis=0, concat_axis=0, tiled=True)]
    ppermute x0 -> x24, starting transfers between devices: none -> 30.3 us  [moved(): lax.ppermute(value, axis, [(i, (i - by) % count) for i in range(count)])]
    pallas_call x3 -> x12, Pallas kernels: 15.6 us -> 42.4 us  [the longest x2 17.9 us: ffn_terms(): pl.pallas_call(ffn_kernel, grid=(6,), in_specs=[whole(half, width), whole...]
    unnamed x63 -> x44, local copies, waits for them, and re-layouts: 30.1 us -> 9.56 us
    all_gather x2, waiting for transfers between devices: 82.3 us -> 101 us  [gather_tiles(): full = lax.all_gather(packed, FS, axis=0, tiled=True)]
    all_to_all x2 -> x0, starting transfers between devices: 9.13 us -> none  [gather_rows(): lax.all_to_all(copies, 'tp', split_axis=0, concat_axis=0, tiled=True)]
  transfers between devices with their start and end apart: 4 -> 26, of which waited for: 3 -> 20; matrix products, arithmetic and copies ran while one was open for 3% -> 1% of each run, Pallas kernels for 3% -> 10%
where the time goes in v2:
time: 264 us; the launch traced here: 263 us
  waiting for transfers between devices  166 us (63%)
  Pallas kernels  42.4 us (16%)
  starting transfers between devices  30.3 us (11%)
  between operations  13.6 us (5%)
  local copies, waits for them, and re-layouts  9.6 us (4%)
    all_gather x2, waiting for transfers between devices, gather_tiles(): full = lax.all_gather(packed, FS, axis=0, tiled=True)  101 us
    ppermute x24, waiting for transfers between devices, moved(): lax.ppermute(value, axis, [(i, (i - by) % count) for i in range(count)])  64.6 us
    ppermute x24, starting transfers between devices, moved(): lax.ppermute(value, axis, [(i, (i - by) % count) for i in range(count)])  30.3 us
    pallas_call x2, Pallas kernels, ffn_terms(): pl.pallas_call(ffn_kernel, grid=(6,), in_specs=[whole(half, width), whole...  17.9 us
    unnamed x44, local copies, waits for them, and re-layouts  9.56 us
    pallas_call x3, Pallas kernels, sent_sums(): pl.pallas_call(pair_sum_kernel, out_shape=[shape] * count, name='pair_sum')  6.86 us
    pallas_call x3, Pallas kernels, combined(): pl.pallas_call(lambda *refs: combine_kernel(half, *refs), out_shape=outs,...  6.65 us
    pallas_call x1, Pallas kernels, mixer_terms(): pl.pallas_call(mixer_kernel, grid=(1,), in_specs=[whole(half, width), who...  5.65 us
  transfers between devices with their start and end apart: 26, of which 20 were waited for; matrix products, arithmetic and copies ran while one was open for 1% of the time, Pallas kernels for 10%

profile of v2, /device:TPU:1, one launch (start us, length us, event | category | flops | bytes accessed | tf_op | source)
XLA Modules:
  0.0 263.0 jit_solution(2549824186123888896)
XLA Ops:
  14.0 2.5 collective-permute-start.1
  18.5 6.7 %collective-permute-done.1 = bf16[48,2048]{1,0:T(8,128)(2,1)S(1)} collective-permute-done((bf16[48,2048]{1,0:T(8,128)(2,1)}, bf16[48,2048]{1,0:T(8,128)(2,1)S(1)}, u32[]{:S(2)}, u32[]{:S(2)}) %collective-permute-start.1) | collective-permute-done | bytes 196640 | tf_op jit(solution)/shard_map/ppermute | solution.py:21
  29.7 94.4 %all-gather.3.cloned.1.call-done = bf16[43008,128]{1,0:T(8,128)(2,1)} async-done(((bf16[1344,128]{1,0:T(8,128)(2,1)}), bf16[43008,128]{1,0:T(8,128)(2,1)}) %all-gather.3.cloned.1.call-update) | async-done | bytes 11010064 | tf_op jit(solution)/shard_map/all_gather | solution.py:126
  124.2 9.0 %ffn.2 = (bf16[192,2048]{1,0:T(8,128)(2,1)S(1)}, bf16[192,2048]{1,0:T(8,128)(2,1)S(1)}) custom-call(bf16[192,2048]{1,0:T(8,128)(2,1)S(1)} %pad_maximum_fusion.mine_ref, bf16[192,2048]{1,0:T(8,128)(2,1)S(1)} %collective-permute-done.3.other_ref, bf16[32,21,64,128]{3,2,1,0:T(8,128)(2,1)} %bitcast.29, bf16[32,21,64,128]{3,2,1,0:T(8,128)(2,1)} %bitcast.30, ...), custom_call_target="tpu_custom_call" | custom-call | tf_op jit(solution)/shard_map/ffn/pallas_call | solution.py:182
  138.3 2.3 pair_sum.3
  141.7 2.4 collective-permute-start.6
  145.3 2.8 %collective-permute-done.5.refs_2_ = bf16[48,2048]{1,0:T(8,128)(2,1)S(1)} collective-permute-done((bf16[48,2048]{1,0:T(8,128)(2,1)}, bf16[48,2048]{1,0:T(8,128)(2,1)S(1)}, u32[]{:S(2)}, u32[]{:S(2)}) %collective-permute-start.5) | collective-permute-done | bytes 196640 | tf_op jit(solution)/shard_map/ppermute | solution.py:21
  148.1 5.1 %collective-permute-done.6.refs_3_ = bf16[48,2048]{1,0:T(8,128)(2,1)S(1)} collective-permute-done((bf16[48,2048]{1,0:T(8,128)(2,1)}, bf16[48,2048]{1,0:T(8,128)(2,1)S(1)}, u32[]{:S(2)}, u32[]{:S(2)}) %collective-permute-start.6) | collective-permute-done | bytes 196640 | tf_op jit(solution)/shard_map/ppermute | solution.py:21
  156.2 2.7 %collective-permute-start.8 = (bf16[48,2048]{1,0:T(8,128)(2,1)}, bf16[48,2048]{1,0:T(8,128)(2,1)S(1)}, u32[]{:S(2)}, u32[]{:S(2)}) collective-permute-start(bf16[48,2048]{1,0:T(8,128)(2,1)} %get-tuple-element.34), channel_id=1, source_target_pairs={{0,6},{2,0},{4,2},{6,4},{1,7},{3,1},{5,3},{7,5},{8,14},{10,8},{12,... | collective-permute-start | bytes 589832 | tf_op jit(solution)/shard_map/ppermute | solution.py:21
  160.5 6.6 %collective-permute-done.8 = bf16[48,2048]{1,0:T(8,128)(2,1)S(1)} collective-permute-done((bf16[48,2048]{1,0:T(8,128)(2,1)}, bf16[48,2048]{1,0:T(8,128)(2,1)S(1)}, u32[]{:S(2)}, u32[]{:S(2)}) %collective-permute-start.8) | collective-permute-done | bytes 196640 | tf_op jit(solution)/shard_map/ppermute | solution.py:21
  167.1 4.5 %collective-permute-done.10 = bf16[48,2048]{1,0:T(8,128)(2,1)S(1)} collective-permute-done((bf16[48,2048]{1,0:T(8,128)(2,1)}, bf16[48,2048]{1,0:T(8,128)(2,1)S(1)}, u32[]{:S(2)}, u32[]{:S(2)}) %collective-permute-start.10) | collective-permute-done | bytes 196640 | tf_op jit(solution)/shard_map/ppermute | solution.py:21
  174.4 5.7 %mixer.1 = (bf16[192,2048]{1,0:T(8,128)(2,1)S(1)}, bf16[192,2048]{1,0:T(8,128)(2,1)S(1)}) custom-call(bf16[192,2048]{1,0:T(8,128)(2,1)S(1)} %constant_dynamic-update-slice_fusion.mine_ref, bf16[192,2048]{1,0:T(8,128)(2,1)S(1)} %collective-permute-done.11.other_ref, bf16[32,21,64,128]{3,2,1,0:T(8,128)(2,1)} %bitcast.32, bf16[32,21,64,128]{3,2,1,0:T(8,128)(2,1)} %bitcast.33, ...), custom_call_target="tpu_custom_call" | custom-call | tf_op jit(solution)/shard_map/mixer/pallas_call | solution.py:312
  184.1 2.3 pair_sum.4
  189.1 9.4 %collective-permute-done.13.refs_2_ = bf16[48,2048]{1,0:T(8,128)(2,1)S(1)} collective-permute-done((bf16[48,2048]{1,0:T(8,128)(2,1)}, bf16[48,2048]{1,0:T(8,128)(2,1)S(1)}, u32[]{:S(2)}, u32[]{:S(2)}) %collective-permute-start.13) | collective-permute-done | bytes 196640 | tf_op jit(solution)/shard_map/ppermute | solution.py:21
  199.5 2.3 combine.4
  201.8 2.5 collective-permute-start.16
  205.9 3.7 %collective-permute-done.16 = bf16[48,2048]{1,0:T(8,128)(2,1)S(1)} collective-permute-done((bf16[48,2048]{1,0:T(8,128)(2,1)}, bf16[48,2048]{1,0:T(8,128)(2,1)S(1)}, u32[]{:S(2)}, u32[]{:S(2)}) %collective-permute-start.16) | collective-permute-done | bytes 196640 | tf_op jit(solution)/shard_map/ppermute | solution.py:21
  211.7 4.9 %collective-permute-done.18 = bf16[48,2048]{1,0:T(8,128)(2,1)S(1)} collective-permute-done((bf16[48,2048]{1,0:T(8,128)(2,1)}, bf16[48,2048]{1,0:T(8,128)(2,1)S(1)}, u32[]{:S(2)}, u32[]{:S(2)}) %collective-permute-start.18) | collective-permute-done | bytes 196640 | tf_op jit(solution)/shard_map/ppermute | solution.py:21
  217.4 6.9 %all-gather.5.cloned.1.call-done = bf16[34816,128]{1,0:T(8,128)(2,1)} async-done(((bf16[1088,128]{1,0:T(8,128)(2,1)}), bf16[34816,128]{1,0:T(8,128)(2,1)}) %all-gather.5.cloned.1.call-update) | async-done | bytes 8912912 | tf_op jit(solution)/shard_map/all_gather | solution.py:126
  224.3 9.0 %ffn.3 = (bf16[192,2048]{1,0:T(8,128)(2,1)S(1)}, bf16[192,2048]{1,0:T(8,128)(2,1)S(1)}) custom-call(bf16[192,2048]{1,0:T(8,128)(2,1)S(1)} %constant_dynamic-update-slice_fusion.4.mine_ref, bf16[192,2048]{1,0:T(8,128)(2,1)S(1)} %collective-permute-done.19.other_ref, bf16[32,17,64,128]{3,2,1,0:T(8,128)(2,1)} %bitcast.37, bf16[32,17,64,128]{3,2,1,0:T(8,128)(2,1)} %bitcast.38, ...), custom_call_target="tpu_custom_call" | custom-call | tf_op jit(solution)/shard_map/ffn/pallas_call | solution.py:182
  238.4 2.3 pair_sum.5
  241.9 2.4 collective-permute-start.22
  245.5 2.7 %collective-permute-done.21.refs_2_ = bf16[48,2048]{1,0:T(8,128)(2,1)S(1)} collective-permute-done((bf16[48,2048]{1,0:T(8,128)(2,1)}, bf16[48,2048]{1,0:T(8,128)(2,1)S(1)}, u32[]{:S(2)}, u32[]{:S(2)}) %collective-permute-start.21) | collective-permute-done | bytes 196640 | tf_op jit(solution)/shard_map/ppermute | solution.py:21
  248.2 5.1 %collective-permute-done.22.refs_3_ = bf16[48,2048]{1,0:T(8,128)(2,1)S(1)} collective-permute-done((bf16[48,2048]{1,0:T(8,128)(2,1)}, bf16[48,2048]{1,0:T(8,128)(2,1)S(1)}, u32[]{:S(2)}, u32[]{:S(2)}) %collective-permute-start.22) | collective-permute-done | bytes 196640 | tf_op jit(solution)/shard_map/ppermute | solution.py:21
  (98 shorter events, 51.3 us)
Async XLA Ops:
  6.5 117.6 %all-gather.3.cloned.1.call-start = ((), (), s32[]{:S(2)}) async-start(), calls=%async_computation | async-start | bytes 11354112 | tf_op jit(solution)/shard_map/all_gather | solution.py:126
  8.4 216.0 %all-gather.5.cloned.1.call-start = ((), (), s32[]{:S(2)}) async-start(), calls=%async_computation.1 | async-start | bytes 9191424 | tf_op jit(solution)/shard_map/all_gather | solution.py:126
  12.0 6.6 %collective-permute-start.2 = (bf16[48,2048]{1,0:T(8,128)(2,1)}, bf16[48,2048]{1,0:T(8,128)(2,1)S(1)}, u32[]{:S(2)}, u32[]{:S(2)}) collective-permute-start(bf16[48,2048]{1,0:T(8,128)(2,1)} %norm.1), channel_id=1, source_target_pairs={{0,2},{2,4},{4,6},{6,0},{1,3},{3,5},{5,7},{7,1},{8,10},{10,12},{12... | collective-permute-start | bytes 589832 | tf_op jit(solution)/shard_map/ppermute | solution.py:21
  14.0 11.2 %collective-permute-start.1 = (bf16[48,2048]{1,0:T(8,128)(2,1)}, bf16[48,2048]{1,0:T(8,128)(2,1)S(1)}, u32[]{:S(2)}, u32[]{:S(2)}) collective-permute-start(bf16[48,2048]{1,0:T(8,128)(2,1)} %norm.1), channel_id=1, source_target_pairs={{0,4},{2,6},{4,0},{6,2},{1,5},{3,7},{5,1},{7,3},{8,12},{10,14},{12... | collective-permute-start | bytes 589832 | tf_op jit(solution)/shard_map/ppermute | solution.py:21
  16.5 8.7 %collective-permute-start = (bf16[48,2048]{1,0:T(8,128)(2,1)}, bf16[48,2048]{1,0:T(8,128)(2,1)S(1)}, u32[]{:S(2)}, u32[]{:S(2)}) collective-permute-start(bf16[48,2048]{1,0:T(8,128)(2,1)} %norm.1), channel_id=1, source_target_pairs={{0,6},{2,0},{4,2},{6,4},{1,7},{3,1},{5,3},{7,5},{8,14},{10,8},{12,... | collective-permute-start | bytes 589832 | tf_op jit(solution)/shard_map/ppermute | solution.py:21
  26.2 3.5 %collective-permute-start.3 = (bf16[192,2048]{1,0:T(8,128)(2,1)S(1)}, bf16[192,2048]{1,0:T(8,128)(2,1)S(1)}, u32[]{:S(2)}, u32[]{:S(2)}) collective-permute-start(bf16[192,2048]{1,0:T(8,128)(2,1)S(1)} %pad_maximum_fusion.mine_ref), channel_id=1, source_target_pairs={{0,1},{1,0},{2,3},{3,2},{4,5},{5,4},{6,7},{7,6},{8,9},{9,8},{10,11... | collective-permute-start | bytes 2359304 | tf_op jit(solution)/shard_map/ppermute | solution.py:21
  134.0 3.3 %collective-permute-start.4 = (bf16[192,2048]{1,0:T(8,128)(2,1)S(1)}, bf16[192,2048]{1,0:T(8,128)(2,1)S(1)}, u32[]{:S(2)}, u32[]{:S(2)}) collective-permute-start(bf16[192,2048]{1,0:T(8,128)(2,1)S(1)} %get-tuple-element.28), channel_id=1, source_target_pairs={{0,1},{1,0},{2,3},{3,2},{4,5},{5,4},{6,7},{7,6},{8,9},{9,8},{10,11... | collective-permute-start | bytes 2359304 | tf_op jit(solution)/shard_map/ppermute | solution.py:21
  140.5 7.6 %collective-permute-start.5 = (bf16[48,2048]{1,0:T(8,128)(2,1)}, bf16[48,2048]{1,0:T(8,128)(2,1)S(1)}, u32[]{:S(2)}, u32[]{:S(2)}) collective-permute-start(bf16[48,2048]{1,0:T(8,128)(2,1)} %get-tuple-element.30), channel_id=1, source_target_pairs={{0,2},{2,4},{4,6},{6,0},{1,3},{3,5},{5,7},{7,1},{8,10},{10,12},{12... | collective-permute-start | bytes 589832 | tf_op jit(solution)/shard_map/ppermute | solution.py:21
  141.7 11.5 %collective-permute-start.6 = (bf16[48,2048]{1,0:T(8,128)(2,1)}, bf16[48,2048]{1,0:T(8,128)(2,1)S(1)}, u32[]{:S(2)}, u32[]{:S(2)}) collective-permute-start(bf16[48,2048]{1,0:T(8,128)(2,1)} %get-tuple-element.31), channel_id=1, source_target_pairs={{0,4},{2,6},{4,0},{6,2},{1,5},{3,7},{5,1},{7,3},{8,12},{10,14},{12... | collective-permute-start | bytes 589832 | tf_op jit(solution)/shard_map/ppermute | solution.py:21
  144.1 9.1 %collective-permute-start.7 = (bf16[48,2048]{1,0:T(8,128)(2,1)}, bf16[48,2048]{1,0:T(8,128)(2,1)S(1)}, u32[]{:S(2)}, u32[]{:S(2)}) collective-permute-start(bf16[48,2048]{1,0:T(8,128)(2,1)} %get-tuple-element.32), channel_id=1, source_target_pairs={{0,6},{2,0},{4,2},{6,4},{1,7},{3,1},{5,3},{7,5},{8,14},{10,8},{12,... | collective-permute-start | bytes 589832 | tf_op jit(solution)/shard_map/ppermute | solution.py:21
  156.2 10.9 %collective-permute-start.8 = (bf16[48,2048]{1,0:T(8,128)(2,1)}, bf16[48,2048]{1,0:T(8,128)(2,1)S(1)}, u32[]{:S(2)}, u32[]{:S(2)}) collective-permute-start(bf16[48,2048]{1,0:T(8,128)(2,1)} %get-tuple-element.34), channel_id=1, source_target_pairs={{0,6},{2,0},{4,2},{6,4},{1,7},{3,1},{5,3},{7,5},{8,14},{10,8},{12,... | collective-permute-start | bytes 589832 | tf_op jit(solution)/shard_map/ppermute | solution.py:21
  158.9 8.2 %collective-permute-start.9 = (bf16[48,2048]{1,0:T(8,128)(2,1)}, bf16[48,2048]{1,0:T(8,128)(2,1)S(1)}, u32[]{:S(2)}, u32[]{:S(2)}) collective-permute-start(bf16[48,2048]{1,0:T(8,128)(2,1)} %get-tuple-element.34), channel_id=1, source_target_pairs={{0,4},{2,6},{4,0},{6,2},{1,5},{3,7},{5,1},{7,3},{8,12},{10,14},{12... | collective-permute-start | bytes 589832 | tf_op jit(solution)/shard_map/ppermute | solution.py:21
  159.3 12.4 %collective-permute-start.10 = (bf16[48,2048]{1,0:T(8,128)(2,1)}, bf16[48,2048]{1,0:T(8,128)(2,1)S(1)}, u32[]{:S(2)}, u32[]{:S(2)}) collective-permute-start(bf16[48,2048]{1,0:T(8,128)(2,1)} %get-tuple-element.34), channel_id=1, source_target_pairs={{0,2},{2,4},{4,6},{6,0},{1,3},{3,5},{5,7},{7,1},{8,10},{10,12},{12... | collective-permute-start | bytes 589832 | tf_op jit(solution)/shard_map/ppermute | solution.py:21
  186.4 12.1 %collective-permute-start.13 = (bf16[48,2048]{1,0:T(8,128)(2,1)}, bf16[48,2048]{1,0:T(8,128)(2,1)S(1)}, u32[]{:S(2)}, u32[]{:S(2)}) collective-permute-start(bf16[48,2048]{1,0:T(8,128)(2,1)} %get-tuple-element.38), channel_id=1, source_target_pairs={{0,2},{2,4},{4,6},{6,0},{1,3},{3,5},{5,7},{7,1},{8,10},{10,12},{12... | collective-permute-start | bytes 589832 | tf_op jit(solution)/shard_map/ppermute | solution.py:21
  186.4 12.1 %collective-permute-start.14 = (bf16[48,2048]{1,0:T(8,128)(2,1)}, bf16[48,2048]{1,0:T(8,128)(2,1)S(1)}, u32[]{:S(2)}, u32[]{:S(2)}) collective-permute-start(bf16[48,2048]{1,0:T(8,128)(2,1)} %get-tuple-element.39), channel_id=1, source_target_pairs={{0,4},{2,6},{4,0},{6,2},{1,5},{3,7},{5,1},{7,3},{8,12},{10,14},{12... | collective-permute-start | bytes 589832 | tf_op jit(solution)/shard_map/ppermute | solution.py:21
  187.5 11.3 %collective-permute-start.15 = (bf16[48,2048]{1,0:T(8,128)(2,1)}, bf16[48,2048]{1,0:T(8,128)(2,1)S(1)}, u32[]{:S(2)}, u32[]{:S(2)}) collective-permute-start(bf16[48,2048]{1,0:T(8,128)(2,1)} %get-tuple-element.40), channel_id=1, source_target_pairs={{0,6},{2,0},{4,2},{6,4},{1,7},{3,1},{5,3},{7,5},{8,14},{10,8},{12,... | collective-permute-start | bytes 589832 | tf_op jit(solution)/shard_map/ppermute | solution.py:21
  201.8 7.8 %collective-permute-start.16 = (bf16[48,2048]{1,0:T(8,128)(2,1)}, bf16[48,2048]{1,0:T(8,128)(2,1)S(1)}, u32[]{:S(2)}, u32[]{:S(2)}) collective-permute-start(bf16[48,2048]{1,0:T(8,128)(2,1)} %get-tuple-element.42), channel_id=1, source_target_pairs={{0,6},{2,0},{4,2},{6,4},{1,7},{3,1},{5,3},{7,5},{8,14},{10,8},{12,... | collective-permute-start | bytes 589832 | tf_op jit(solution)/shard_map/ppermute | solution.py:21
  204.4 7.3 %collective-permute-start.17 = (bf16[48,2048]{1,0:T(8,128)(2,1)}, bf16[48,2048]{1,0:T(8,128)(2,1)S(1)}, u32[]{:S(2)}, u32[]{:S(2)}) collective-permute-start(bf16[48,2048]{1,0:T(8,128)(2,1)} %get-tuple-element.42), channel_id=1, source_target_pairs={{0,4},{2,6},{4,0},{6,2},{1,5},{3,7},{5,1},{7,3},{8,12},{10,14},{12... | collective-permute-start | bytes 589832 | tf_op jit(solution)/shard_map/ppermute | solution.py:21
  204.4 12.3 %collective-permute-start.18 = (bf16[48,2048]{1,0:T(8,128)(2,1)}, bf16[48,2048]{1,0:T(8,128)(2,1)S(1)}, u32[]{:S(2)}, u32[]{:S(2)}) collective-permute-start(bf16[48,2048]{1,0:T(8,128)(2,1)} %get-tuple-element.42), channel_id=1, source_target_pairs={{0,2},{2,4},{4,6},{6,0},{1,3},{3,5},{5,7},{7,1},{8,10},{10,12},{12... | collective-permute-start | bytes 589832 | tf_op jit(solution)/shard_map/ppermute | solution.py:21
  216.7 7.7 %collective-permute-start.19 = (bf16[192,2048]{1,0:T(8,128)(2,1)S(1)}, bf16[192,2048]{1,0:T(8,128)(2,1)S(1)}, u32[]{:S(2)}, u32[]{:S(2)}) collective-permute-start(bf16[192,2048]{1,0:T(8,128)(2,1)S(1)} %constant_dynamic-update-slice_fusion.4.mine_ref), channel_id=1, source_target_pairs={{0,1},{1,0},{2,3},{3,2},{4,5},{5,4},{6,7},{7,6},{8,9},{9,8},{10,11... | collective-permute-start | bytes 2359304 | tf_op jit(solution)/shard_map/ppermute | solution.py:21
  234.2 3.3 %collective-permute-start.20 = (bf16[192,2048]{1,0:T(8,128)(2,1)S(1)}, bf16[192,2048]{1,0:T(8,128)(2,1)S(1)}, u32[]{:S(2)}, u32[]{:S(2)}) collective-permute-start(bf16[192,2048]{1,0:T(8,128)(2,1)S(1)} %get-tuple-element.44), channel_id=1, source_target_pairs={{0,1},{1,0},{2,3},{3,2},{4,5},{5,4},{6,7},{7,6},{8,9},{9,8},{10,11... | collective-permute-start | bytes 2359304 | tf_op jit(solution)/shard_map/ppermute | solution.py:21
  240.7 7.5 %collective-permute-start.21 = (bf16[48,2048]{1,0:T(8,128)(2,1)}, bf16[48,2048]{1,0:T(8,128)(2,1)S(1)}, u32[]{:S(2)}, u32[]{:S(2)}) collective-permute-start(bf16[48,2048]{1,0:T(8,128)(2,1)} %get-tuple-element.46), channel_id=1, source_target_pairs={{0,2},{2,4},{4,6},{6,0},{1,3},{3,5},{5,7},{7,1},{8,10},{10,12},{12... | collective-permute-start | bytes 589832 | tf_op jit(solution)/shard_map/ppermute | solution.py:21
  241.9 11.4 %collective-permute-start.22 = (bf16[48,2048]{1,0:T(8,128)(2,1)}, bf16[48,2048]{1,0:T(8,128)(2,1)S(1)}, u32[]{:S(2)}, u32[]{:S(2)}) collective-permute-start(bf16[48,2048]{1,0:T(8,128)(2,1)} %get-tuple-element.47), channel_id=1, source_target_pairs={{0,4},{2,6},{4,0},{6,2},{1,5},{3,7},{5,1},{7,3},{8,12},{10,14},{12... | collective-permute-start | bytes 589832 | tf_op jit(solution)/shard_map/ppermute | solution.py:21
  244.3 9.1 %collective-permute-start.23 = (bf16[48,2048]{1,0:T(8,128)(2,1)}, bf16[48,2048]{1,0:T(8,128)(2,1)S(1)}, u32[]{:S(2)}, u32[]{:S(2)}) collective-permute-start(bf16[48,2048]{1,0:T(8,128)(2,1)} %get-tuple-element.48), channel_id=1, source_target_pairs={{0,6},{2,0},{4,2},{6,4},{1,7},{3,1},{5,3},{7,5},{8,14},{10,8},{12,... | collective-permute-start | bytes 589832 | tf_op jit(solution)/shard_map/ppermute | solution.py:21
  (21 other events, 112.0 us)
Sparse Core Ops, SparseCore 0:
  9.9 114.2 all-gather.2
  126.7 97.5 all-gather.4
